TPU v7x, 32 devices: a whole 2x2x4 slice. The times are simulated.
32 devices in a mesh: sp: 8 (over z, y), tp: 4 (over x, core).
Axes of the slice: x: 2, y: 2, z: 4, core: 2. Of those that a mesh axis runs over, the one named last changes fastest.
Arguments:
- stream: bfloat16 [16384, 4096], P('sp', 'tp'), may hold values from -18 to 18
- doc_ids: int32 [16384], P('sp'), may hold values from 0 to 1, never falling along the last dimension, each value on 1 to 12288 neighbouring positions
- norm_gain: bfloat16 [3, 4096], replicated, may hold values from 0.099609375 to 1.8984375
- proj_in: bfloat16 [3, 4096, 1024], P(None, 'tp', 'sp'), may hold values from -0.09375 to 0.09375
- mix_pool: bfloat16 [3, 8, 128, 128], replicated, may hold values from -0.5 to 0.5
- pool_gain: bfloat16 [3, 1024], replicated, may hold values from 0.099609375 to 1.8984375
- proj_out: bfloat16 [3, 1024, 4096], P(None, 'sp', 'tp'), may hold values from -0.1875 to 0.1875
Outputs:
- stream_out: bfloat16 [16384, 4096], P('sp', 'tp')
Inputs may be any that keep to these rules, and one draw needn't show every extreme that they name: `doc_ids`: document numbers never fall along the sequence; each document holds 1 to 12288 positions, one exactly that many.
All inputs are finite; a program needn't handle non-finite values.
Results may differ from a plain program's by a relative error of at most 0.02.
Values may be sent and summed in bfloat16 or wider, within the bound.
A program may use at most 64 MiB of HBM per device.

v0:
```python
import jax
import jax.numpy as jnp
from jax import lax
from jax.sharding import PartitionSpec as P

epsilon = 1e-06
span_reach = 15


def shifted(value, axis, steps):
    count = lax.axis_size(axis)
    initial, last = (max(0, -steps), min(count, count - steps))
    return lax.ppermute(value, axis, [(source, source + steps) for source in range(initial, last)])


def span_pool(padded, labels, widths):
    kept = padded.shape[0] - span_reach
    own_label = labels[span_reach:]
    summed = jnp.zeros((kept, padded.shape[1]), jnp.float32)
    counted = jnp.zeros((kept, padded.shape[1]), jnp.float32)
    for offset in range(span_reach + 1):
        first = span_reach - offset
        member = (labels[first : first + kept] == own_label)[:, None] & (offset < widths)[None, :]
        factor = member.astype(jnp.float32)
        summed = summed + padded[first : first + kept] * factor
        counted = counted + factor
    return summed / counted - padded[span_reach:]


def body(stream, doc_ids, norm_gain, proj_in, mix_pool, pool_gain, proj_out):
    width_dev = stream.shape[1]
    tp_count = lax.axis_size("tp")
    model_width = width_dev * tp_count
    group_size = mix_pool.shape[2]
    channels = proj_in.shape[2] * lax.axis_size("sp")
    local = channels // tp_count
    groups_dev = local // group_size
    column = lax.axis_index("tp")
    chan_ids = column * local + jnp.arange(local, dtype=jnp.int32)
    widths = jnp.left_shift(jnp.int32(2), chan_ids // group_size % 4)
    labels = (doc_ids + 1).astype(jnp.bfloat16)
    hidden_state = stream
    layer_count = proj_in.shape[0]
    in_whole, out_whole = (
        lax.all_gather(proj_in, "sp", axis=2, tiled=True),
        lax.all_gather(proj_out, "sp", axis=1, tiled=True),
    )
    for layer in range(layer_count):
        row_count = hidden_state.shape[0]
        wide = hidden_state.astype(jnp.float32)
        own_squares = jnp.sum(wide * wide, axis=1)
        gain = lax.dynamic_slice_in_dim(norm_gain[layer], column * width_dev, width_dev).astype(
            jnp.float32
        )
        gained = (wide * gain[None, :]).astype(jnp.bfloat16)
        partial_value = jnp.dot(gained, in_whole[layer], preferred_element_type=jnp.float32)
        squares = lax.psum(own_squares, "tp")
        summed_in = lax.psum_scatter(
            partial_value.astype(jnp.bfloat16), "tp", scatter_dimension=1, tiled=True
        ).astype(jnp.float32)
        row_scale = lax.rsqrt(squares / model_width + epsilon)
        mixed_in = (summed_in * row_scale[:, None]).astype(jnp.bfloat16)
        before, before_labels = shifted((mixed_in[-span_reach:], labels[-span_reach:]), "sp", 1)
        padded = jnp.concatenate([before, mixed_in], axis=0).astype(jnp.float32)
        tags = jnp.concatenate([before_labels, labels], axis=0)
        pooled = span_pool(padded, tags, widths).astype(jnp.bfloat16)
        grouped = pooled.reshape(row_count, groups_dev, group_size)
        mixing = lax.dynamic_slice_in_dim(mix_pool[layer], column * groups_dev, groups_dev, 0)
        blended = jnp.einsum(
            "tgc,gcd->tgd", grouped, mixing, preferred_element_type=jnp.float32
        ).reshape(row_count, local)
        scale = lax.dynamic_slice_in_dim(pool_gain[layer], column * local, local).astype(
            jnp.float32
        )
        mixed = (blended * scale[None, :]).astype(jnp.bfloat16)
        full_mixed = lax.all_gather(mixed, "tp", axis=1, tiled=True)
        update = jnp.dot(full_mixed, out_whole[layer], preferred_element_type=jnp.float32)
        hidden_state = (wide + update).astype(jnp.bfloat16)
    return hidden_state


def solution(mesh):
    in_specs = (P("sp", "tp"), P("sp"), P(), P(None, "tp", "sp"), P(), P(), P(None, "sp", "tp"))
    out_specs = P("sp", "tp")
    return jax.shard_map(body, mesh=mesh, in_specs=in_specs, out_specs=out_specs, check_vma=False)
```

profile of v0, /device:TPU:0, one launch (start us, length us, event | category | flops | bytes accessed | tf_op | source)
XLA Modules:
  0.0 557.2 jit_solution(6840634323078287556)
XLA Ops:
  7.3 6.4 %copy.8 = bf16[2048,1024]{0,1:T(8,128)(2,1)} copy(bf16[2048,1024]{1,0:T(8,128)(2,1)} %param.7) | data formatting | bytes 8388608 | tf_op args[0]
  13.8 97.8 %all-gather.6.cloned.1.call-done = bf16[3,1024,1024]{2,1,0:T(8,128)(2,1)} async-done(((bf16[3,1024,128]{2,1,0:T(8,128)(2,1)}), bf16[3,1024,1024]{2,1,0:T(8,128)(2,1)}) %all-gather.6.cloned.1.call-update) | async-done | bytes 6291472 | tf_op jit(solution)/shard_map/all_gather | solution.py:45
  111.6 9.6 %fusion.18 = bf16[2048,1024]{1,0:T(8,128)(2,1)} fusion(bf16[2048,1024]{0,1:T(8,128)(2,1)} %copy.8, f32[1024]{0:T(1024)S(1)} %bitcast.87, bf16[3,1024,1024]{2,1,0:T(8,128)(2,1)} %all-gather.6.cloned.1.call-done), kind=kOutput, calls=%fused_computation.24 | convolution fusion | flops 4303355904 | bytes 10489856 | tf_op jit(solution)/shard_map/dot_general | solution.py:56
  125.5 3.6 fusion.1
  129.2 6.1 %psum.21 = f32[2048]{0:T(1024)S(1)} all-reduce(f32[2048]{0:T(1024)S(1)} %fusion.1), channel_id=1, replica_groups=mesh['sp'=8,'tp'=4] {'tp'}, use_global_device_ids=true, to_apply=%region_2.3 | all-reduce | flops 2048 | bytes 16384 | tf_op jit(solution)/shard_map/psum | solution.py:57
  135.7 28.3 %reduce-scatter.4.cloned.1.call-done = bf16[2048,256]{1,0:T(8,128)(2,1)} async-done(((bf16[2048,1024]{1,0:T(8,128)(2,1)}), bf16[2048,256]{1,0:T(8,128)(2,1)}) %reduce-scatter.4.cloned.1.call-update) | async-done | bytes 1048592 | tf_op jit(solution)/shard_map/reduce_scatter | solution.py:58
  170.5 9.9 %fusion.105 = f32[2,128,2048]{2,1,0:T(8,128)S(1)} fusion(bf16[1,8,128,128]{3,2,1,0:T(8,128)(2,1)S(1)} %get-tuple-element.8, s32[]{:T(128)S(6)} %select_n.125, f32[2063,256]{1,0:T(8,128)S(1)} %maximum_convert_fusion, pred[256]{0:T(512)(128)(4,1)S(1)} %get-tuple-element.35, pred[2048]{0:T(1024)(128)(4,1)S(1)} %get-tuple-element.29, ...), kind=kOutput, calls=%fused_computation.184 | convolution fusion | flops 176685056 | bytes 35758084 | tf_op jit(solution)/shard_map/tgc,gcd->tgd/dot_general | solution.py:69
  181.9 83.0 %all-gather.10.cloned.1.call-done = bf16[3,1024,1024]{2,1,0:T(8,128)(2,1)} async-done(((bf16[3,128,1024]{2,1,0:T(8,128)(2,1)}), bf16[3,1024,1024]{2,1,0:T(8,128)(2,1)}) %all-gather.10.cloned.1.call-update) | async-done | bytes 6291472 | tf_op jit(solution)/shard_map/all_gather | solution.py:46
  264.9 34.1 %all-gather.8.cloned.1.call-done = bf16[2048,1024]{0,1:T(8,128)(2,1)} async-done(((bf16[2048,256]{0,1:T(8,128)(2,1)}), bf16[2048,1024]{0,1:T(8,128)(2,1)}) %all-gather.8.cloned.1.call-update) | async-done | bytes 4194320 | tf_op jit(solution)/shard_map/all_gather | solution.py:76
  299.0 9.2 %fusion.4 = (f32[2048]{0:T(1024)S(1)}, bf16[2048,1024]{0,1:T(8,128)(2,1)S(1)}) fusion(bf16[2048,1024]{0,1:T(8,128)(2,1)} %all-gather.8.cloned.1.call-done, bf16[3,1024,1024]{2,1,0:T(8,128)(2,1)} %all-gather.10.cloned.1.call-done, bf16[2048,1024]{0,1:T(8,128)(2,1)} %copy.8), kind=kOutput, calls=%fused_computation.13 | convolution fusion | flops 4307548160 | bytes 14688256 | tf_op jit(solution)/shard_map/dot_general | solution.py:77
  310.1 8.0 %fusion.21 = bf16[2048,1024]{1,0:T(8,128)(2,1)} fusion(bf16[2048,1024]{0,1:T(8,128)(2,1)S(1)} %get-tuple-element.32, f32[1024]{0:T(1024)S(1)} %bitcast.85, bf16[3,1024,1024]{2,1,0:T(8,128)(2,1)} %all-gather.6.cloned.1.call-done), kind=kOutput, calls=%fused_computation.25 | convolution fusion | flops 4303355904 | bytes 10489856 | tf_op jit(solution)/shard_map/dot_general | solution.py:56
  318.3 6.0 %psum.22 = f32[2048]{0:T(1024)S(1)} all-reduce(f32[2048]{0:T(1024)S(1)} %get-tuple-element.31), channel_id=1, replica_groups=mesh['sp'=8,'tp'=4] {'tp'}, use_global_device_ids=true, to_apply=%region_5.6 | all-reduce | flops 2048 | bytes 16384 | tf_op jit(solution)/shard_map/psum | solution.py:57
  324.3 38.5 %reduce-scatter.6.cloned.1.call-done = bf16[2048,256]{1,0:T(8,128)(2,1)} async-done(((bf16[2048,1024]{1,0:T(8,128)(2,1)}), bf16[2048,256]{1,0:T(8,128)(2,1)}) %reduce-scatter.6.cloned.1.call-update) | async-done | bytes 1048592 | tf_op jit(solution)/shard_map/reduce_scatter | solution.py:58
  364.3 3.8 collective-permute-start.2
  369.3 9.9 %fusion.102 = f32[2,128,2048]{2,1,0:T(8,128)S(1)} fusion(bf16[1,8,128,128]{3,2,1,0:T(8,128)(2,1)S(1)} %get-tuple-element.9, s32[]{:T(128)S(6)} %select_n.125, f32[2063,256]{1,0:T(8,128)S(1)} %maximum_convert_fusion.1, pred[256]{0:T(512)(128)(4,1)S(1)} %get-tuple-element.35, pred[2048]{0:T(1024)(128)(4,1)S(1)} %get-tuple-element.29, ...), kind=kOutput, calls=%fused_computation.181 | convolution fusion | flops 176685056 | bytes 35758084 | tf_op jit(solution)/shard_map/tgc,gcd->tgd/dot_general | solution.py:69
  380.6 35.2 %all-gather.12.cloned.1.call-done = bf16[2048,1024]{0,1:T(8,128)(2,1)} async-done(((bf16[2048,256]{0,1:T(8,128)(2,1)}), bf16[2048,1024]{0,1:T(8,128)(2,1)}) %all-gather.12.cloned.1.call-update) | async-done | bytes 4194320 | tf_op jit(solution)/shard_map/all_gather | solution.py:76
  415.8 9.2 %fusion.7 = (f32[2048]{0:T(1024)S(1)}, bf16[2048,1024]{0,1:T(8,128)(2,1)S(1)}) fusion(bf16[2048,1024]{0,1:T(8,128)(2,1)} %all-gather.12.cloned.1.call-done, bf16[3,1024,1024]{2,1,0:T(8,128)(2,1)} %all-gather.10.cloned.1.call-done, bf16[2048,1024]{0,1:T(8,128)(2,1)} %copy-done.5), kind=kOutput, calls=%fused_computation.16 | convolution fusion | flops 4307548160 | bytes 14688256 | tf_op jit(solution)/shard_map/dot_general | solution.py:77
  427.0 8.0 %fusion.24 = bf16[2048,1024]{1,0:T(8,128)(2,1)} fusion(bf16[2048,1024]{0,1:T(8,128)(2,1)S(1)} %get-tuple-element.34, f32[1024]{0:T(1024)S(1)} %bitcast.86, bf16[3,1024,1024]{2,1,0:T(8,128)(2,1)} %all-gather.6.cloned.1.call-done), kind=kOutput, calls=%fused_computation.26 | convolution fusion | flops 4303355904 | bytes 10489856 | tf_op jit(solution)/shard_map/dot_general | solution.py:56
  435.1 6.0 %psum.23 = f32[2048]{0:T(1024)S(1)} all-reduce(f32[2048]{0:T(1024)S(1)} %get-tuple-element.33), channel_id=1, replica_groups=mesh['sp'=8,'tp'=4] {'tp'}, use_global_device_ids=true, to_apply=%region_8.9 | all-reduce | flops 2048 | bytes 16384 | tf_op jit(solution)/shard_map/psum | solution.py:57
  441.1 38.5 %reduce-scatter.8.cloned.1.call-done = bf16[2048,256]{1,0:T(8,128)(2,1)} async-done(((bf16[2048,1024]{1,0:T(8,128)(2,1)}), bf16[2048,256]{1,0:T(8,128)(2,1)}) %reduce-scatter.8.cloned.1.call-update) | async-done | bytes 1048592 | tf_op jit(solution)/shard_map/reduce_scatter | solution.py:58
  486.2 9.9 %fusion.99 = f32[2,128,2048]{2,1,0:T(8,128)S(1)} fusion(bf16[1,8,128,128]{3,2,1,0:T(8,128)(2,1)S(1)} %get-tuple-element.7, s32[]{:T(128)S(6)} %select_n.125, f32[2063,256]{1,0:T(8,128)S(1)} %maximum_convert_fusion.2, pred[256]{0:T(512)(128)(4,1)S(1)} %get-tuple-element.35, pred[2048]{0:T(1024)(128)(4,1)S(1)} %get-tuple-element.29, ...), kind=kOutput, calls=%fused_computation.178 | convolution fusion | flops 176685056 | bytes 35758084 | tf_op jit(solution)/shard_map/tgc,gcd->tgd/dot_general | solution.py:69
  497.2 35.4 %all-gather.14.cloned.1.call-done = bf16[2048,1024]{0,1:T(8,128)(2,1)} async-done(((bf16[2048,256]{0,1:T(8,128)(2,1)}), bf16[2048,1024]{0,1:T(8,128)(2,1)}) %all-gather.14.cloned.1.call-update) | async-done | bytes 4194320 | tf_op jit(solution)/shard_map/all_gather | solution.py:76
  532.7 11.0 %fusion.8 = bf16[2048,1024]{0,1:T(8,128)(2,1)} fusion(bf16[2048,1024]{0,1:T(8,128)(2,1)} %copy-done.4, bf16[2048,1024]{0,1:T(8,128)(2,1)} %all-gather.14.cloned.1.call-done, bf16[3,1024,1024]{2,1,0:T(8,128)(2,1)} %all-gather.10.cloned.1.call-done), kind=kOutput, calls=%fused_computation.17 | convolution fusion | flops 4301258752 | bytes 14680064 | tf_op jit(solution)/shard_map/dot_general | solution.py:77
  543.7 6.4 %copy.16 = bf16[2048,1024]{1,0:T(8,128)(2,1)} copy(bf16[2048,1024]{0,1:T(8,128)(2,1)} %fusion.8) | data formatting | bytes 8388608 | tf_op jit(solution)/shard_map/convert_element_type | solution.py:78
  (71 shorter events, 29.2 us)
Async XLA Ops:
  6.5 105.1 %all-gather.6.cloned.1.call-start = ((), (), s32[]{:S(2)}) async-start(), calls=%async_computation.3 | async-start | bytes 7077888 | tf_op jit(solution)/shard_map/all_gather | solution.py:45
  7.3 156.7 %reduce-scatter.4.cloned.1.call-start = ((), (), s32[]{:S(2)}) async-start(), calls=%async_computation.4 | async-start | bytes 5242880 | tf_op jit(solution)/shard_map/reduce_scatter | solution.py:58
  7.3 6.4 %copy-start.1 = (bf16[3,4096]{1,0:T(4,128)(2,1)S(1)}, bf16[3,4096]{1,0:T(4,128)(2,1)}, u32[]{:S(2)}) copy-start(bf16[3,4096]{1,0:T(4,128)(2,1)} %param.9) | copy-start | bytes 73732
  121.2 0.8 copy-start.3
  121.3 143.7 %all-gather.10.cloned.1.call-start = ((), (), s32[]{:S(2)}) async-start(), calls=%async_computation.6 | async-start | bytes 7077888 | tf_op jit(solution)/shard_map/all_gather | solution.py:46
  122.0 177.0 %all-gather.8.cloned.1.call-start = ((), (), s32[]{:S(2)}) async-start(), calls=%async_computation.5 | async-start | bytes 5242880 | tf_op jit(solution)/shard_map/all_gather | solution.py:76
  122.1 13.5 %collective-permute-start.1 = (bf16[15]{0:T(256)(128)(2,1)S(1)}, bf16[15]{0:T(256)(128)(2,1)S(1)}, u32[]{:S(2)}, u32[]{:S(2)}) collective-permute-start(bf16[15]{0:T(256)(128)(2,1)S(1)} %slice.366), channel_id=1, source_target_pairs={{0,4},{4,8},{8,12},{12,16},{16,20},{20,24},{24,28},{1,5},{5,9},{9,... | collective-permute-start | bytes 98 | tf_op jit(solution)/shard_map/ppermute | solution.py:13
  125.5 10.0 %copy-start.2 = (bf16[3,1024]{1,0:T(4,128)(2,1)S(1)}, bf16[3,1024]{1,0:T(4,128)(2,1)}, u32[]{:S(2)}) copy-start(bf16[3,1024]{1,0:T(4,128)(2,1)} %param.12) | copy-start | bytes 18436
  125.5 10.0 %copy-start = (bf16[3,8,128,128]{3,2,1,0:T(8,128)(2,1)S(1)}, bf16[3,8,128,128]{3,2,1,0:T(8,128)(2,1)}, u32[]{:S(2)}) copy-start(bf16[3,8,128,128]{3,2,1,0:T(8,128)(2,1)} %param.11) | copy-start | bytes 2359300
  165.6 4.7 collective-permute-start
  181.6 181.1 %reduce-scatter.6.cloned.1.call-start = ((), (), s32[]{:S(2)}) async-start(), calls=%async_computation.7 | async-start | bytes 5242880 | tf_op jit(solution)/shard_map/reduce_scatter | solution.py:58
  308.2 2.0 copy-start.5
  318.2 97.6 %all-gather.12.cloned.1.call-start = ((), (), s32[]{:S(2)}) async-start(), calls=%async_computation.8 | async-start | bytes 5242880 | tf_op jit(solution)/shard_map/all_gather | solution.py:76
  364.3 4.7 collective-permute-start.2
  380.4 99.3 %reduce-scatter.8.cloned.1.call-start = ((), (), s32[]{:S(2)}) async-start(), calls=%async_computation.9 | async-start | bytes 5242880 | tf_op jit(solution)/shard_map/reduce_scatter | solution.py:58
  425.0 2.0 copy-start.4
  435.1 97.6 %all-gather.14.cloned.1.call-start = ((), (), s32[]{:S(2)}) async-start(), calls=%async_computation.10 | async-start | bytes 5242880 | tf_op jit(solution)/shard_map/all_gather | solution.py:76
  481.2 4.7 collective-permute-start.3
Sparse Core Ops, SparseCore 0:
  9.4 102.1 all-gather.5
  121.4 42.5 reduce-scatter.3
  166.2 98.6 all-gather.9
  266.3 32.6 all-gather.7
  318.3 44.3 reduce-scatter.5
  380.5 35.2 all-gather.11
  435.2 44.3 reduce-scatter.7
  497.4 35.2 all-gather.13
where the time goes:
time: 563 us; the launch traced here: 557 us
  waiting for transfers between devices  395 us (70%)
  matrix products  84.7 us (15%)
  blocking collectives  18.1 us (3%)
  local copies, waits for them, and re-layouts  17 us (3%)
  starting transfers between devices  14.9 us (3%)
  between operations  14.1 us (3%)
  other arithmetic  12.9 us (2%)
    reduce_scatter x3, waiting for transfers between devices, body(): lax.psum_scatter(partial_value.astype(jnp.bfloat16), 'tp', scatter_dimens...  105 us
    all_gather x3, waiting for transfers between devices, body(): full_mixed = lax.all_gather(mixed, 'tp', axis=1, tiled=True)  105 us
    all_gather x1, waiting for transfers between devices, body(): lax.all_gather(proj_in, 'sp', axis=2, tiled=True)  97.8 us
    all_gather x1, waiting for transfers between devices, body(): lax.all_gather(proj_out, 'sp', axis=1, tiled=True)  83 us
    dot_general x3, matrix products, body(): jnp.einsum('tgc,gcd->tgd', grouped, mixing, preferred_element_type=jnp.fl...  29.7 us
    dot_general x3, matrix products, body(): jnp.dot(full_mixed, out_whole[layer], preferred_element_type=jnp.float32)  29.4 us
    dot_general x3, matrix products, body(): jnp.dot(gained, in_whole[layer], preferred_element_type=jnp.float32)  25.7 us
    psum x3, blocking collectives, body(): squares = lax.psum(own_squares, 'tp')  18.1 us
  transfers between devices with their start and end apart: 12, of which 11 were waited for; matrix products, arithmetic and copies ran while one was open for 4% of the time, Pallas kernels for 0%

commit v1 on v0

--- a/solution.py
+++ b/solution.py
@@ -1,9 +1,362 @@
+import functools
+
 import jax
 import jax.numpy as jnp
 from jax import lax
+from jax.experimental import pallas as pl
+from jax.experimental.pallas import tpu as pltpu
 from jax.sharding import PartitionSpec as P
 
-epsilon = 1e-06
+EPSILON = 1e-06
+HALO = 16
+CHUNKS = 8
+LAG = 4
+MESH = pl.DeviceIdType.MESH
+F32, BF16 = jnp.float32, jnp.bfloat16
+
+
+def mixer(sp, tp, snake, x_ref, pos_ref, gain_ref, win_ref, mix_ref, pgain_ref, wout_ref, o_ref,
+          win, wout, send1, own1, recv1, sum2, recv2, mixed, zbuf, hrecv,
+          sq_own, sq_in1, sq_sum, sq_in2,
+          ring_s, ring_r, s1, r1, s2, r2, s3, r3, hs, hr):
+    layers, model_dev, chan_dev = win_ref.shape
+    tokens = x_ref.shape[0]
+    rows = tokens // CHUNKS
+    channels = chan_dev * sp
+    half = channels // 2
+    group = mix_ref.shape[-1]
+    model = model_dev * tp
+    row_dev = wout_ref.shape[1]
+    s, t = lax.axis_index("sp"), lax.axis_index("tp")
+    core = lax.rem(t, 2)
+    partner = t + 1 - 2 * core
+    across = lax.rem(t + 2, tp)
+
+    def place(device):
+        if not snake:
+            return device
+        z, y = device // 2, lax.rem(device, 2)
+        return z * (1 - y) + (sp - 1 - z) * y
+
+    def device_at(place):
+        if not snake:
+            return place
+        up = place // (sp // 2)
+        return 2 * (place * (1 - up) + (sp - 1 - place) * up) + up
+
+    here = place(s)
+    after, before = device_at(lax.rem(here + 1, sp)), device_at(lax.rem(here + sp - 1, sp))
+    following, leading = lax.rem(s + 1, sp), lax.rem(s + sp - 1, sp)
+
+    barrier = pltpu.get_barrier_semaphore()
+    for peer in ({"tp": partner}, {"tp": across}, {"sp": after}, {"sp": before}, {"sp": following}, {"sp": leading}):
+        pl.semaphore_signal(barrier, inc=1, device_id=peer, device_id_type=MESH)
+    pl.semaphore_wait(barrier, 6)
+
+    ahead = sp // 2
+    back = sp - 1 - ahead
+
+    def ring_view(layer, side, piece, source, own):
+        if side == 0:
+            part = model_dev // 2
+            cut = pl.ds(piece * part, part)
+            target = win.at[layer, cut, pl.ds(pl.multiple_of(source * chan_dev, chan_dev), chan_dev)]
+            return (win_ref.at[layer, cut] if own else target), target
+        part = row_dev // 2
+        target = wout.at[layer, pl.ds(pl.multiple_of(source * row_dev + piece * part, part), part)]
+        return (wout_ref.at[layer, pl.ds(piece * part, part)] if own else target), target
+
+    def ring_copy(layer, side, piece, way, hop, own):
+        origin = here - hop + sp if way == 0 else here + hop
+        source = device_at(lax.rem(origin, sp))
+        src, dst = ring_view(layer, side, piece, source, own)
+        return pltpu.make_async_remote_copy(
+            src_ref=src, dst_ref=dst,
+            send_sem=ring_s.at[layer, side, piece, way, hop], recv_sem=ring_r.at[layer, side, piece, way, hop],
+            device_id={"sp": after if way == 0 else before}, device_id_type=MESH)
+
+    def ring_land(layer, side, piece, way, hop):
+        origin = here - hop - 1 + 2 * sp if way == 0 else here + hop + 1
+        _, dst = ring_view(layer, side, piece, device_at(lax.rem(origin, sp)), False)
+        return pltpu.make_async_remote_copy(
+            src_ref=dst, dst_ref=dst,
+            send_sem=ring_s.at[layer, side, piece, way, hop], recv_sem=ring_r.at[layer, side, piece, way, hop],
+            device_id={"sp": after if way == 0 else before}, device_id_type=MESH)
+
+    def ring_start(layer, side, piece):
+        for way in range(2):
+            if (ahead, back)[way] > 0:
+                ring_copy(layer, side, piece, way, 0, True).start()
+
+    def ring_step(layer, side, piece, hop):
+        for way, hops in ((0, ahead), (1, back)):
+            @pl.when(hop < hops)
+            def _():
+                ring_land(layer, side, piece, way, hop).wait_recv()
+
+            @pl.when(hop + 1 < hops)
+            def _():
+                ring_copy(layer, side, piece, way, hop + 1, False).start()
+
+    item_count = 2 * layers
+    per_step = -(-ahead // (CHUNKS // 2))
+    item_steps = -(-ahead // per_step)
+
+    def pump(step, piece):
+        item = 1 + step // item_steps
+        layer, side = item // 2, lax.rem(item, 2)
+
+        @pl.when(item < item_count)
+        def _():
+            for which in range(2):
+                @pl.when(side == which)
+                def _():
+                    for j in range(per_step):
+                        hop = lax.rem(step, item_steps) * per_step + j
+                        if ahead % per_step == 0:
+                            ring_step(layer, which, piece, hop)
+                        else:
+                            @pl.when(hop < ahead)
+                            def _():
+                                ring_step(layer, which, piece, hop)
+
+        following_item = item + 1
+
+        @pl.when((following_item < item_count) & (lax.rem(step, item_steps) == max(item_steps - 2, 0)))
+        def _():
+            for which in range(2):
+                @pl.when(lax.rem(following_item, 2) == which)
+                def _():
+                    ring_start(following_item // 2, which, piece)
+
+    for piece in range(2):
+        ring_start(0, 0, piece)
+    for layer in range(layers):
+        win[layer, :, pl.ds(pl.multiple_of(s * chan_dev, chan_dev), chan_dev)] = win_ref[layer]
+        wout[layer, pl.ds(pl.multiple_of(s * row_dev, row_dev), row_dev), :] = wout_ref[layer]
+
+    @pl.loop(0, CHUNKS)
+    def _(i):
+        at = pl.ds(pl.multiple_of(i * rows, rows), rows)
+        o_ref[at] = x_ref[at]
+
+    @pl.loop(0, ahead)
+    def _(hop):
+        for piece in range(2):
+            ring_step(0, 0, piece, hop)
+            @pl.when(hop == max(ahead - 2, 0))
+            def _():
+                ring_start(0, 1, piece)
+
+    def split(step):
+        layer = step // CHUNKS
+        return layer, CHUNKS - 1 - lax.rem(step, CHUNKS)
+
+    def copy1(i):
+        return [pltpu.make_async_remote_copy(
+            src_ref=a, dst_ref=b, send_sem=s1.at[j, i], recv_sem=r1.at[j, i],
+            device_id={"tp": partner}, device_id_type=MESH)
+            for j, (a, b) in enumerate(((send1.at[i], recv1.at[i]), (sq_own.at[i], sq_in1.at[i])))]
+
+    def copy2(layer, i):
+        par = lax.rem(layer, 2)
+        return [pltpu.make_async_remote_copy(
+            src_ref=a, dst_ref=b, send_sem=s2.at[j, i], recv_sem=r2.at[j, par, i],
+            device_id={"tp": across}, device_id_type=MESH)
+            for j, (a, b) in enumerate(((sum2.at[i], recv2.at[par, i]), (sq_sum.at[i], sq_in2.at[par, i])))]
+
+    def copy3(i, side):
+        view = mixed.at[i, :, pl.ds(pl.multiple_of(side * half, half), half)]
+        return pltpu.make_async_remote_copy(
+            src_ref=view, dst_ref=view, send_sem=s3.at[i], recv_sem=r3.at[i],
+            device_id={"tp": partner}, device_id_type=MESH)
+
+    def halo_copy(layer):
+        return pltpu.make_async_remote_copy(
+            src_ref=zbuf.at[pl.ds(tokens, HALO)], dst_ref=hrecv.at[layer], send_sem=hs.at[layer], recv_sem=hr.at[layer],
+            device_id={"sp": following}, device_id_type=MESH)
+
+    def project(step):
+        layer, i = split(step)
+        at = pl.ds(pl.multiple_of(i * rows, rows), rows)
+        wide = o_ref[at].astype(F32)
+        squares = wide * wide
+        lanes = squares[:, :128]
+        for j in range(1, model_dev // 128):
+            lanes = lanes + squares[:, j * 128:(j + 1) * 128]
+        sq_own[i] = jnp.sum(lanes.T.reshape(16, 8, rows), axis=0)
+        gained = (wide * gain_ref[layer]).astype(BF16)
+        other = pl.ds(pl.multiple_of((1 - core) * half, half), half)
+        send1[i] = jnp.dot(gained, win[layer, :, other], preferred_element_type=F32).astype(BF16)
+        for c in copy1(i):
+            c.start()
+        mine = pl.ds(pl.multiple_of(core * half, half), half)
+        own1[i] = jnp.dot(gained, win[layer, :, mine], preferred_element_type=F32).astype(BF16)
+
+    def join(step):
+        layer, i = split(step)
+        for c in copy1(i):
+            c.wait()
+        sum2[i] = (own1[i].astype(F32) + recv1[i].astype(F32)).astype(BF16)
+        sq_sum[i] = sq_own[i] + sq_in1[i]
+        for c in copy2(layer, i):
+            c.start()
+
+    def normalise(step):
+        layer, i = split(step)
+        par = lax.rem(layer, 2)
+        for c in copy2(layer, i):
+            c.wait()
+
+        @pl.when(i == CHUNKS - 2)
+        def _():
+            halo_copy(layer).wait_send()
+
+        total = jnp.sum(sq_sum[i] + sq_in2[par, i], axis=0, keepdims=True)
+        scale = jnp.broadcast_to(lax.rsqrt(total / model + EPSILON), (128, rows)).T
+        at = pl.ds(pl.multiple_of(HALO + i * rows, HALO), rows)
+        for j in range(half // 128):
+            cols = slice(j * 128, (j + 1) * 128)
+            zbuf[at, cols] = ((sum2[i, :, cols].astype(F32) + recv2[par, i, :, cols].astype(F32)) * scale).astype(BF16)
+
+        @pl.when(i == CHUNKS - 1)
+        def _():
+            halo_copy(layer).start()
+
+    def pool(step):
+        layer, i = split(step)
+
+        @pl.when(i == 0)
+        def _():
+            halo_copy(layer).wait_recv()
+            zbuf[pl.ds(0, HALO)] = hrecv[layer]
+
+        wide_at = pl.ds(pl.multiple_of(i * rows, HALO), rows + HALO)
+        pos = pos_ref[wide_at]
+        for g in range(half // group):
+            cols = slice(g * group, (g + 1) * group)
+            z = zbuf[wide_at, cols].astype(F32)
+            window = 2 ** (1 + g % 4)
+            total = z
+            step_rows = 1
+            while step_rows < window:
+                total = total + jnp.where(pos >= step_rows, pltpu.roll(total, step_rows, 0), 0.0)
+                step_rows *= 2
+            count = jnp.minimum(pos[HALO:] + 1.0, float(window))
+            pooled = (total[HALO:] / count - z[HALO:]).astype(BF16)
+            blended = jnp.dot(pooled, mix_ref[layer, g], preferred_element_type=F32)
+            place_at = pl.ds(pl.multiple_of(core * half + g * group, group), group)
+            mixed[i, :, place_at] = (blended * pgain_ref[layer, :, cols]).astype(BF16)
+        copy3(i, core).start()
+
+    def finish(step):
+        layer, i = split(step)
+        copy3(i, core).wait_send()
+        copy3(i, 1 - core).wait_recv()
+        at = pl.ds(pl.multiple_of(i * rows, rows), rows)
+        for j in range(2):
+            cols = slice(j * (model_dev // 2), (j + 1) * (model_dev // 2))
+            update = jnp.dot(mixed[i], wout[layer, :, cols], preferred_element_type=F32)
+            o_ref[at, cols] = (o_ref[at, cols].astype(F32) + update).astype(BF16)
+
+    steps = layers * CHUNKS
+
+    @pl.loop(0, steps + LAG)
+    def _(k):
+        pump(k, 0)
+
+        @pl.when(k < steps)
+        def _():
+            project(k)
+
+        pump(k, 1)
+
+        @pl.when((k >= LAG - 1) & (k < steps + LAG - 1))
+        def _():
+            normalise(k - (LAG - 1))
+
+        @pl.when(k >= LAG)
+        def _():
+            pool(k - LAG)
+
+        @pl.when(k < steps)
+        def _():
+            join(k)
+
+        @pl.when(k >= LAG)
+        def _():
+            finish(k - LAG)
+
+    @pl.loop(0, layers)
+    def _(layer):
+        for side in range(2):
+            for piece in range(2):
+                for way, hops in ((0, ahead), (1, back)):
+                    @pl.loop(0, hops)
+                    def _(hop):
+                        ring_copy(layer, side, piece, way, hop, False).wait_send()
+
+
+def distances(doc_ids, sp):
+    labels = doc_ids + 1
+    reach = 2 * HALO
+    earlier = lax.ppermute(labels[-reach:], "sp", [(i, i + 1) for i in range(sp - 1)])
+    padded = jnp.concatenate([earlier, labels])
+    kept = labels.shape[0] + HALO
+    own = padded[HALO:]
+    same = jnp.zeros((kept,), F32)
+    for offset in range(1, HALO):
+        same = same + (padded[HALO - offset:HALO - offset + kept] == own).astype(F32)
+    return jnp.broadcast_to(same[:, None], (kept, 128))
+
+
+def body(snake, sp, tp, stream, doc_ids, norm_gain, proj_in, mix_pool, pool_gain, proj_out):
+    layers, model_dev, chan_dev = proj_in.shape
+    tokens = stream.shape[0]
+    rows = tokens // CHUNKS
+    channels = chan_dev * sp
+    half = channels // 2
+    groups = mix_pool.shape[1] // 2
+    t = lax.axis_index("tp")
+    core = t % 2
+    gain = lax.dynamic_slice_in_dim(norm_gain, t * model_dev, model_dev, 1).astype(F32)[:, None, :]
+    mix = lax.dynamic_slice_in_dim(mix_pool, core * groups, groups, 1)
+    pgain = lax.dynamic_slice_in_dim(pool_gain, core * half, half, 1).astype(F32)[:, None, :]
+    pos = distances(doc_ids, sp)
+    hops = sp // 2
+    dma, vmem = pltpu.SemaphoreType.DMA, pltpu.VMEM
+    return pl.pallas_call(
+        functools.partial(mixer, sp, tp, snake),
+        out_shape=jax.ShapeDtypeStruct(stream.shape, BF16),
+        in_specs=[pl.BlockSpec(memory_space=pltpu.VMEM)] * 7,
+        out_specs=pl.BlockSpec(memory_space=pltpu.VMEM),
+        scratch_shapes=[
+            vmem((layers, model_dev, channels), BF16),
+            vmem((layers, channels, model_dev), BF16),
+            vmem((CHUNKS, rows, half), BF16),
+            vmem((CHUNKS, rows, half), BF16),
+            vmem((CHUNKS, rows, half), BF16),
+            vmem((CHUNKS, rows, half), BF16),
+            vmem((2, CHUNKS, rows, half), BF16),
+            vmem((CHUNKS, rows, channels), BF16),
+            vmem((HALO + tokens, half), BF16),
+            vmem((layers, HALO, half), BF16),
+            vmem((CHUNKS, 8, rows), F32),
+            vmem((CHUNKS, 8, rows), F32),
+            vmem((CHUNKS, 8, rows), F32),
+            vmem((2, CHUNKS, 8, rows), F32),
+            dma((layers, 2, 2, 2, hops)),
+            dma((layers, 2, 2, 2, hops)),
+            dma((2, CHUNKS)), dma((2, CHUNKS)),
+            dma((2, CHUNKS)), dma((2, 2, CHUNKS)),
+            dma((CHUNKS,)), dma((CHUNKS,)),
+            dma((layers,)), dma((layers,)),
+        ],
+        compiler_params=pltpu.CompilerParams(
+            collective_id=0, has_side_effects=True, vmem_limit_bytes=60 * 2**20),
+    )(stream, pos, gain, proj_in, mix, pgain, proj_out)
+
+
 span_reach = 15
 
 
@@ -27,7 +380,7 @@
     return summed / counted - padded[span_reach:]
 
 
-def body(stream, doc_ids, norm_gain, proj_in, mix_pool, pool_gain, proj_out):
+def plain_body(stream, doc_ids, norm_gain, proj_in, mix_pool, pool_gain, proj_out):
     width_dev = stream.shape[1]
     tp_count = lax.axis_size("tp")
     model_width = width_dev * tp_count
@@ -58,7 +411,7 @@
         summed_in = lax.psum_scatter(
             partial_value.astype(jnp.bfloat16), "tp", scatter_dimension=1, tiled=True
         ).astype(jnp.float32)
-        row_scale = lax.rsqrt(squares / model_width + epsilon)
+        row_scale = lax.rsqrt(squares / model_width + EPSILON)
         mixed_in = (summed_in * row_scale[:, None]).astype(jnp.bfloat16)
         before, before_labels = shifted((mixed_in[-span_reach:], labels[-span_reach:]), "sp", 1)
         padded = jnp.concatenate([before, mixed_in], axis=0).astype(jnp.float32)
@@ -80,6 +433,13 @@
 
 
 def solution(mesh):
+    sp, tp = mesh.shape["sp"], mesh.shape["tp"]
     in_specs = (P("sp", "tp"), P("sp"), P(), P(None, "tp", "sp"), P(), P(), P(None, "sp", "tp"))
-    out_specs = P("sp", "tp")
-    return jax.shard_map(body, mesh=mesh, in_specs=in_specs, out_specs=out_specs, check_vma=False)
+
+    def whole(stream, doc_ids, norm_gain, proj_in, mix_pool, pool_gain, proj_out):
+        fits = tp == 4 and sp % 2 == 0 and proj_in.shape[2] // sp % 128 == 0 and mix_pool.shape[1] % 8 == 0
+        part = functools.partial(body, True, sp, tp) if fits else plain_body
+        return jax.shard_map(part, mesh=mesh, in_specs=in_specs, out_specs=P("sp", "tp"), check_vma=False)(
+            stream, doc_ids, norm_gain, proj_in, mix_pool, pool_gain, proj_out)
+
+    return whole

time: 563 us -> 209 us (0.37)
  waiting for transfers between devices: 395 us -> 0.01 us
  Pallas kernels: 0 us -> 193 us
  matrix products: 84.7 us -> 0 us
  blocking collectives: 18.1 us -> 0 us
  between operations: 14.1 us -> 0.05 us
  other arithmetic: 12.9 us -> 2.3 us
  starting transfers between devices: 14.9 us -> 4.89 us
  local copies, waits for them, and re-layouts: 17 us -> 8 us
    all_gather x5 -> x0, waiting for transfers between devices: 286 us -> none  [the longest x3 105 us: body(): full_mixed = lax.all_gather(mixed, 'tp', axis=1, tiled=True)]
    pallas_call x0 -> x1, Pallas kernels: none -> 193 us  [body(): pl.pallas_call(functools.partial(mixer, sp, tp, snake), out_shape=jax.Sha...]
    reduce_scatter x3 -> x0, waiting for transfers between devices: 105 us -> none  [body(): lax.psum_scatter(partial_value.astype(jnp.bfloat16), 'tp', scatter_dimens...]
    dot_general x9 -> x0, matrix products: 84.7 us -> none  [the longest x3 29.7 us: body(): jnp.einsum('tgc,gcd->tgd', grouped, mixing, preferred_element_type=jnp.fl...]
    psum x3 -> x0, blocking collectives: 18.1 us -> none  [body(): squares = lax.psum(own_squares, 'tp')]
    ppermute x4 -> x1, starting transfers between devices: 14.3 us -> 4.89 us  [distances(): lax.ppermute(labels[-reach:], 'sp', [(i, i + 1) for i in range(sp - 1)])]
    convert_element_type x9 -> x0, other arithmetic: 8.78 us -> none  [the longest x3 4.68 us: body(): mixed_in = (summed_in * row_scale[:, None]).astype(jnp.bfloat16)]
    convert_element_type x1 -> x0, local copies, waits for them, and re-layouts: 6.39 us -> none  [body(): hidden_state = (wide + update).astype(jnp.bfloat16)]
  transfers between devices with their start and end apart: 12 -> 1, of which waited for: 11 -> 0; matrix products, arithmetic and copies ran while one was open for 4% -> 2% of each run, Pallas kernels for 0% -> 0%
where the time goes in v1:
time: 209 us; the launch traced here: 208 us
  Pallas kernels  193 us (92%)
  local copies, waits for them, and re-layouts  8 us (4%)
  starting transfers between devices  4.89 us (2%)
  other arithmetic  2.3 us (1%)
    pallas_call x1, Pallas kernels, body(): pl.pallas_call(functools.partial(mixer, sp, tp, snake), out_shape=jax.Sha...  193 us
    ppermute x1, starting transfers between devices, distances(): lax.ppermute(labels[-reach:], 'sp', [(i, i + 1) for i in range(sp - 1)])  4.89 us
    unnamed x3, local copies, waits for them, and re-layouts  4.65 us
  transfers between devices with their start and end apart: 1, of which 0 were waited for; matrix products, arithmetic and copies ran while one was open for 2% of the time, Pallas kernels for 0%

profile of v1, /device:TPU:0, one launch (start us, length us, event | category | flops | bytes accessed | tf_op | source)
XLA Modules:
  0.0 208.3 jit_solution(84374939285252941)
XLA Ops:
  0.0 0.0 copy-start
  0.0 0.8 broadcast_add_fusion
  0.8 0.1 slice.68
  0.9 4.9 %collective-permute-start = (s32[32]{0:T(128)S(1)}, s32[32]{0:T(128)S(1)}, u32[]{:S(2)}, u32[]{:S(2)}) collective-permute-start(s32[32]{0:T(128)S(1)} %slice.68), channel_id=1, source_target_pairs={{0,4},{4,8},{8,12},{12,16},{16,20},{20,24},{24,28},{1,5},{5,9},{9,... | collective-permute-start | bytes 392 | tf_op jit(solution)/shard_map/ppermute | solution.py:303
  5.8 0.7 dynamic-slice_convert_fusion.1
  6.5 0.7 dynamic-slice_convert_fusion
  7.2 0.0 copy-done
  7.2 0.8 constant_dynamic-slice_fusion.mix_ref
  7.9 0.6 reshape.2.pgain_ref
  8.5 0.6 reshape.1.gain_ref
  9.1 0.0 collective-permute-done
  9.1 0.1 convert_add_fusion
  9.3 1.3 broadcast_in_dim.16.pos_ref
  10.6 193.0 %shard_map.73 = bf16[2048,1024]{1,0:T(8,128)(2,1)} custom-call(bf16[2048,1024]{1,0:T(8,128)(2,1)} %x_ref.1, f32[2064,128]{1,0:T(8,128)} %broadcast_in_dim.16.pos_ref, f32[3,1,1024]{2,1,0:T(1,128)} %reshape.1.gain_ref, bf16[3,1024,128]{2,1,0:T(8,128)(2,1)} %win_ref.1, bf16[3,4,128,128]{3,2,1,0:T(8,128)(2,1)} %constant_dynamic-slice_fusion.mix_ref, ...), custom_call_target="tpu_custom_call" | custom-call | tf_op jit(solution)/shard_map/pallas_call | solution.py:328
  203.6 4.6 %copy.9 = bf16[2048,1024]{1,0:T(8,128)(2,1)} copy(bf16[2048,1024]{1,0:T(8,128)(2,1)} %shard_map.73) | data formatting | bytes 8388608
Async XLA Ops:
  0.0 7.2 %copy-start = (bf16[3,8,128,128]{3,2,1,0:T(8,128)(2,1)S(1)}, bf16[3,8,128,128]{3,2,1,0:T(8,128)(2,1)}, u32[]{:S(2)}) copy-start(bf16[3,8,128,128]{3,2,1,0:T(8,128)(2,1)} %param.11) | copy-start | bytes 2359300
  0.9 8.3 %collective-permute-start = (s32[32]{0:T(128)S(1)}, s32[32]{0:T(128)S(1)}, u32[]{:S(2)}, u32[]{:S(2)}) collective-permute-start(s32[32]{0:T(128)S(1)} %slice.68), channel_id=1, source_target_pairs={{0,4},{4,8},{8,12},{12,16},{16,20},{20,24},{24,28},{1,5},{5,9},{9,... | collective-permute-start | bytes 392 | tf_op jit(solution)/shard_map/ppermute | solution.py:303

commit v2 on v1

--- a/solution.py
+++ b/solution.py
@@ -15,9 +15,10 @@
 F32, BF16 = jnp.float32, jnp.bfloat16
 
 
-def mixer(sp, tp, snake, x_ref, pos_ref, gain_ref, win_ref, mix_ref, pgain_ref, wout_ref, o_ref,
+def mixer(sp, tp, snake, x_ref, doc_ref, gains_ref, win_ref, mix_ref, pgains_ref, wout_ref, o_ref,
           win, wout, send1, own1, recv1, sum2, recv2, mixed, zbuf, hrecv,
           sq_own, sq_in1, sq_sum, sq_in2,
+          labels, before_labels, pos_ref, gain_ref, pgain_ref, ls, lr,
           ring_s, ring_r, s1, r1, s2, r2, s3, r3, hs, hr):
     layers, model_dev, chan_dev = win_ref.shape
     tokens = x_ref.shape[0]
@@ -54,7 +55,9 @@
     pl.semaphore_wait(barrier, 6)
 
     ahead = sp // 2
-    back = sp - 1 - ahead
+
+    def hops(way, piece):
+        return ahead if way == piece else ahead - 1
 
     def ring_view(layer, side, piece, source, own):
         if side == 0:
@@ -85,16 +88,16 @@
 
     def ring_start(layer, side, piece):
         for way in range(2):
-            if (ahead, back)[way] > 0:
+            if hops(way, piece) > 0:
                 ring_copy(layer, side, piece, way, 0, True).start()
 
     def ring_step(layer, side, piece, hop):
-        for way, hops in ((0, ahead), (1, back)):
-            @pl.when(hop < hops)
+        for way in range(2):
+            @pl.when(hop < hops(way, piece))
             def _():
                 ring_land(layer, side, piece, way, hop).wait_recv()
 
-            @pl.when(hop + 1 < hops)
+            @pl.when(hop + 1 < hops(way, piece))
             def _():
                 ring_copy(layer, side, piece, way, hop + 1, False).start()
 
@@ -131,14 +134,37 @@
 
     for piece in range(2):
         ring_start(0, 0, piece)
+    reach = 2 * HALO
+    documents = doc_ref[...].astype(F32)
+    for j in range(tokens // 128):
+        labels[pl.ds(reach + j * 128, 128)] = jnp.broadcast_to(documents[j:j + 1], (128, 128)).T
+    label_copy = pltpu.make_async_remote_copy(
+        src_ref=labels.at[pl.ds(tokens, reach)], dst_ref=before_labels, send_sem=ls, recv_sem=lr,
+        device_id={"sp": following}, device_id_type=MESH)
+    label_copy.start()
     for layer in range(layers):
         win[layer, :, pl.ds(pl.multiple_of(s * chan_dev, chan_dev), chan_dev)] = win_ref[layer]
         wout[layer, pl.ds(pl.multiple_of(s * row_dev, row_dev), row_dev), :] = wout_ref[layer]
-
-    @pl.loop(0, CHUNKS)
-    def _(i):
+        own_gain = gains_ref[:, pl.ds(pl.multiple_of(t * model_dev, model_dev), model_dev)].astype(F32)
+        gain_ref[layer] = own_gain[layer:layer + 1]
+        own_gain = pgains_ref[:, pl.ds(pl.multiple_of(core * half, half), half)].astype(F32)
+        pgain_ref[layer] = own_gain[layer:layer + 1]
+
+    def distances(ext):
+        same = jnp.zeros((ext.shape[0] - HALO, 128), F32)
+        for offset in range(1, HALO):
+            same = same + (pltpu.roll(ext, offset, 0) == ext)[HALO:].astype(F32)
+        return same
+
+    label_copy.wait()
+    labels[pl.ds(0, reach)] = jnp.where(s == 0, -1.0, before_labels[...])
+    pos_ref[pl.ds(0, HALO)] = distances(labels[pl.ds(0, reach)])
+
+    def prepare(i):
         at = pl.ds(pl.multiple_of(i * rows, rows), rows)
         o_ref[at] = x_ref[at]
+        pos_ref[pl.ds(pl.multiple_of(HALO + i * rows, HALO), rows)] = distances(
+            labels[pl.ds(pl.multiple_of(HALO + i * rows, HALO), rows + HALO)])
 
     @pl.loop(0, ahead)
     def _(hop):
@@ -147,6 +173,12 @@
             @pl.when(hop == max(ahead - 2, 0))
             def _():
                 ring_start(0, 1, piece)
+
+        share = -(-CHUNKS // ahead)
+        for j in range(share):
+            @pl.when(hop * share + j < CHUNKS)
+            def _():
+                prepare(hop * share + j)
 
     def split(step):
         layer = step // CHUNKS
@@ -244,7 +276,7 @@
                 step_rows *= 2
             count = jnp.minimum(pos[HALO:] + 1.0, float(window))
             pooled = (total[HALO:] / count - z[HALO:]).astype(BF16)
-            blended = jnp.dot(pooled, mix_ref[layer, g], preferred_element_type=F32)
+            blended = jnp.dot(pooled, mix_ref[layer, core * (half // group) + g], preferred_element_type=F32)
             place_at = pl.ds(pl.multiple_of(core * half + g * group, group), group)
             mixed[i, :, place_at] = (blended * pgain_ref[layer, :, cols]).astype(BF16)
         copy3(i, core).start()
@@ -291,23 +323,10 @@
     def _(layer):
         for side in range(2):
             for piece in range(2):
-                for way, hops in ((0, ahead), (1, back)):
-                    @pl.loop(0, hops)
+                for way in range(2):
+                    @pl.loop(0, hops(way, piece))
                     def _(hop):
                         ring_copy(layer, side, piece, way, hop, False).wait_send()
-
-
-def distances(doc_ids, sp):
-    labels = doc_ids + 1
-    reach = 2 * HALO
-    earlier = lax.ppermute(labels[-reach:], "sp", [(i, i + 1) for i in range(sp - 1)])
-    padded = jnp.concatenate([earlier, labels])
-    kept = labels.shape[0] + HALO
-    own = padded[HALO:]
-    same = jnp.zeros((kept,), F32)
-    for offset in range(1, HALO):
-        same = same + (padded[HALO - offset:HALO - offset + kept] == own).astype(F32)
-    return jnp.broadcast_to(same[:, None], (kept, 128))
 
 
 def body(snake, sp, tp, stream, doc_ids, norm_gain, proj_in, mix_pool, pool_gain, proj_out):
@@ -316,13 +335,6 @@
     rows = tokens // CHUNKS
     channels = chan_dev * sp
     half = channels // 2
-    groups = mix_pool.shape[1] // 2
-    t = lax.axis_index("tp")
-    core = t % 2
-    gain = lax.dynamic_slice_in_dim(norm_gain, t * model_dev, model_dev, 1).astype(F32)[:, None, :]
-    mix = lax.dynamic_slice_in_dim(mix_pool, core * groups, groups, 1)
-    pgain = lax.dynamic_slice_in_dim(pool_gain, core * half, half, 1).astype(F32)[:, None, :]
-    pos = distances(doc_ids, sp)
     hops = sp // 2
     dma, vmem = pltpu.SemaphoreType.DMA, pltpu.VMEM
     return pl.pallas_call(
@@ -345,6 +357,12 @@
             vmem((CHUNKS, 8, rows), F32),
             vmem((CHUNKS, 8, rows), F32),
             vmem((2, CHUNKS, 8, rows), F32),
+            vmem((2 * HALO + tokens, 128), F32),
+            vmem((2 * HALO, 128), F32),
+            vmem((HALO + tokens, 128), F32),
+            vmem((layers, 1, model_dev), F32),
+            vmem((layers, 1, half), F32),
+            dma, dma,
             dma((layers, 2, 2, 2, hops)),
             dma((layers, 2, 2, 2, hops)),
             dma((2, CHUNKS)), dma((2, CHUNKS)),
@@ -354,7 +372,7 @@
         ],
         compiler_params=pltpu.CompilerParams(
             collective_id=0, has_side_effects=True, vmem_limit_bytes=60 * 2**20),
-    )(stream, pos, gain, proj_in, mix, pgain, proj_out)
+    )(stream, doc_ids.reshape(-1, 128), norm_gain, proj_in, mix_pool, pool_gain, proj_out)
 
 
 span_reach = 15

time: 209 us -> 194 us (0.928)
  starting transfers between devices: 4.89 us -> 0 us
  local copies, waits for them, and re-layouts: 8 us -> 4.64 us
  Pallas kernels: 193 us -> 190 us
  other arithmetic: 2.3 us -> 0 us
    ppermute x1 -> x0, starting transfers between devices: 4.89 us -> none  [distances(): lax.ppermute(labels[-reach:], 'sp', [(i, i + 1) for i in range(sp - 1)])]
    pallas_call x1, Pallas kernels: 193 us -> 190 us  [body(): pl.pallas_call(functools.partial(mixer, sp, tp, snake), out_shape=jax.Sha...]
    broadcast_in_dim x3 -> x0, local copies, waits for them, and re-layouts: 2.51 us -> none  [the longest x1 1.31 us: distances(): return jnp.broadcast_to(same[:, None], (kept, 128))]
    unnamed x3 -> x1, local copies, waits for them, and re-layouts: 4.65 us -> 4.64 us
  transfers between devices with their start and end apart: 1 -> 0, of which waited for: 0 -> 0; matrix products, arithmetic and copies ran while one was open for 2% -> 0% of each run, Pallas kernels for 0% -> 0%
where the time goes in v2:
time: 194 us
  Pallas kernels  190 us (98%)
  local copies, waits for them, and re-layouts  4.64 us (2%)
    pallas_call x1, Pallas kernels, body(): pl.pallas_call(functools.partial(mixer, sp, tp, snake), out_shape=jax.Sha...  190 us
    unnamed x1, local copies, waits for them, and re-layouts  4.64 us

profile of v2, /device:TPU:0, one launch (start us, length us, event | category | flops | bytes accessed | tf_op | source)
XLA Modules:
  0.0 194.3 jit_solution(17263384590089187185)
XLA Ops:
  0.0 189.7 %shard_map.73 = bf16[2048,1024]{1,0:T(8,128)(2,1)} custom-call(bf16[2048,1024]{1,0:T(8,128)(2,1)} %x_ref.1, s32[16,128]{1,0:T(8,128)} %bitcast.1, bf16[3,4096]{1,0:T(4,128)(2,1)} %gains_ref.1, bf16[3,1024,128]{2,1,0:T(8,128)(2,1)} %win_ref.1, bf16[3,8,128,128]{3,2,1,0:T(8,128)(2,1)} %mix_ref.1, bf16[3,1024]{1,0:T(4,128)(2,1)} %pgains_ref.1, ...), custom_call_target="tpu_custom_call" | custom-call | tf_op jit(solution)/shard_map/pallas_call | solution.py:340
  189.7 4.6 %copy.9 = bf16[2048,1024]{1,0:T(8,128)(2,1)} copy(bf16[2048,1024]{1,0:T(8,128)(2,1)} %shard_map.73) | data formatting | bytes 8388608
